TPU v7x, 32 devices: a whole 2x2x4 slice. The times are simulated.
32 devices in a mesh: sp: 8 (over z, y), tp: 4 (over x, core).
Axes of the slice: x: 2, y: 2, z: 4, core: 2. Of those that a mesh axis runs over, the one named last changes fastest.
Arguments:
- resid: bfloat16 [2048, 2048], P(('sp', 'tp')), may hold values from -6 to 6
- query_a: bfloat16 [2048, 4, 128], P('sp', 'tp')
- key_a: bfloat16 [2048, 4, 128], P('sp', 'tp')
- value_a: bfloat16 [2048, 4, 128], P('sp', 'tp'), may hold values from -6 to 6
- query_b: bfloat16 [2048, 4, 256], P('sp', 'tp')
- key_b: bfloat16 [2048, 4, 256], P('sp', 'tp')
- value_b: bfloat16 [2048, 4, 128], P('sp', 'tp'), may hold values from -6 to 6
- lambda_a: float32 [4], P('tp'), may hold values from 0.3 to 0.8
- lambda_b: float32 [4], P('tp'), may hold values from 0.3 to 0.8
- head_gain: float32 [128], replicated, may hold values from 0.1 to 1.9
- out_weight: bfloat16 [1024, 2048], replicated, may hold values from -0.1875 to 0.1875
- norm_gain: float32 [2048], replicated, may hold values from 0.1 to 1.9
- expert_ids: int32 [2048, 4], P(('sp', 'tp')), may hold values from 0 to 31, all different within a row; in each aligned block of 64 rows (0 to 63, 64 to 127, ...) at most 16 rows name the same one
- expert_mix: float32 [2048, 4], P(('sp', 'tp')), may hold values from 0.2 to 1
- gate_experts: bfloat16 [32, 2048, 1024], P(('sp', 'tp')), may hold values from -0.125 to 0.125
- up_experts: bfloat16 [32, 2048, 1024], P(('sp', 'tp')), may hold values from -0.125 to 0.125
- down_experts: bfloat16 [32, 1024, 2048], P(('sp', 'tp')), may hold values from -0.1875 to 0.1875
- shared_gate: bfloat16 [2048, 512], replicated, may hold values from -0.125 to 0.125
- shared_up: bfloat16 [2048, 512], replicated, may hold values from -0.125 to 0.125
- shared_down: bfloat16 [512, 2048], replicated, may hold values from -0.25 to 0.25
Outputs:
- layer_out: bfloat16 [2048, 2048], P(('sp', 'tp'))
Inputs may be any that keep to these rules, and one draw needn't show every extreme that they name: `expert_ids`: in each aligned block of 64 rows (the rows of one device) no expert is named more than 16 times, a bound that some block reaches.
All inputs are finite; a program needn't handle non-finite values.
Results may differ from a plain program's by a relative error of at most 0.017.
Values may be sent and summed in bfloat16 or wider, within the bound.
No kernel may reach another device: no remote copies, remote signals or barrier semaphores. Data moves between devices by JAX's collectives and lax.ppermute only.
A program may use at most 128 MiB of HBM per device.

v0:
```python
import math
import jax
import jax.numpy as jnp
from jax import lax
from jax.sharding import PartitionSpec as P

NEG_FILL = -1e30
EPSILON = 1e-05
HEAD_SCALE = 0.8
KEY_SPAN = 2048


def swiglu_rows(row_set, w_gate, w_up, w_down):
    gate_val = jnp.dot(row_set, w_gate, preferred_element_type=jnp.float32)
    up_val = jnp.dot(row_set, w_up, preferred_element_type=jnp.float32)
    hidden = (jax.nn.silu(gate_val) * up_val).astype(jnp.bfloat16)
    return jnp.dot(hidden, w_down, preferred_element_type=jnp.float32)


def online_update(state, query_map, key_map, value_block, causal, scaling):
    row_top, denoms, numerator = state
    scores = (
        jnp.einsum("qhd,khd->hqk", query_map, key_map, preferred_element_type=jnp.float32) * scaling
    )
    scores = jnp.where(causal, scores, NEG_FILL)
    new_top = jnp.maximum(row_top, jnp.max(scores, axis=2))
    exponent = jnp.where(causal, jnp.exp(scores - new_top[:, :, None]), 0.0)
    shrink = jnp.exp(row_top - new_top)
    denoms = denoms * shrink + jnp.sum(exponent, axis=2)
    numerator = numerator * jnp.transpose(shrink)[:, :, None] + jnp.einsum(
        "hqk,khe->qhe",
        exponent.astype(jnp.bfloat16),
        value_block,
        preferred_element_type=jnp.float32,
    )
    return (new_top, denoms, numerator)


def group_update(states, queries, key_block, value_block, causal):
    map_width = queries.shape[2] // 2
    scaling = map_width ** (-0.5)
    first_state = online_update(
        states[0],
        queries[:, :, :map_width],
        key_block[:, :, :map_width],
        value_block,
        causal,
        scaling,
    )
    second_state = online_update(
        states[1],
        queries[:, :, map_width:],
        key_block[:, :, map_width:],
        value_block,
        causal,
        scaling,
    )
    return (first_state, second_state)


def empty_state(query_rows, head_count, value_width):
    single = (
        jnp.full((head_count, query_rows), NEG_FILL, jnp.float32),
        jnp.zeros((head_count, query_rows), jnp.float32),
        jnp.zeros((query_rows, head_count, value_width), jnp.float32),
    )
    return (single, single)


def finish_group(states, lambdas, head_gain):
    first_out = states[0][2] / jnp.transpose(states[0][1])[:, :, None]
    second_out = states[1][2] / jnp.transpose(states[1][1])[:, :, None]
    differ = first_out - lambdas[None, :, None] * second_out
    scale_rms = lax.rsqrt(jnp.mean(differ * differ, axis=2, keepdims=True) + EPSILON)
    return (differ * scale_rms * head_gain[None, None, :] * HEAD_SCALE).astype(jnp.bfloat16)


def per_device(
    resid,
    query_a,
    key_a,
    value_a,
    query_b,
    key_b,
    value_b,
    lambda_a,
    lambda_b,
    head_gain,
    out_weight,
    norm_gain,
    expert_ids,
    expert_mix,
    gate_experts,
    up_experts,
    down_experts,
    shared_gate,
    shared_up,
    shared_down,
):
    query_rows = query_a.shape[0]
    value_width = value_a.shape[2]
    query_pos = lax.axis_index("sp") * query_rows + jnp.arange(query_rows, dtype=jnp.int32)
    start_state = (
        empty_state(query_rows, query_a.shape[1], value_width),
        empty_state(query_rows, query_b.shape[1], value_width),
    )
    key_piece_a = lax.all_gather(key_a, "sp", axis=0, tiled=True)
    value_piece_a = lax.all_gather(value_a, "sp", axis=0, tiled=True)
    key_piece_b = lax.all_gather(key_b, "sp", axis=0, tiled=True)
    value_piece_b = lax.all_gather(value_b, "sp", axis=0, tiled=True)
    piece_rows = key_piece_a.shape[0]
    step_rows = math.gcd(piece_rows, KEY_SPAN)

    def one_step(step_index, inner_state):
        begin_row = step_index * step_rows
        key_pos = begin_row + jnp.arange(step_rows, dtype=jnp.int32)
        causal = (key_pos[None, :] <= query_pos[:, None])[None]
        part_a = group_update(
            inner_state[0],
            query_a,
            lax.dynamic_slice_in_dim(key_piece_a, begin_row, step_rows, 0),
            lax.dynamic_slice_in_dim(value_piece_a, begin_row, step_rows, 0),
            causal,
        )
        part_b = group_update(
            inner_state[1],
            query_b,
            lax.dynamic_slice_in_dim(key_piece_b, begin_row, step_rows, 0),
            lax.dynamic_slice_in_dim(value_piece_b, begin_row, step_rows, 0),
            causal,
        )
        return (part_a, part_b)

    state_a, state_b = lax.fori_loop(0, piece_rows // step_rows, one_step, start_state)
    heads_a = finish_group(state_a, lambda_a, head_gain)
    heads_b = finish_group(state_b, lambda_b, head_gain)
    tok_dev = resid.shape[0]
    back_a, back_b = (
        lax.all_to_all(heads_a, "tp", split_axis=0, concat_axis=1, tiled=True),
        lax.all_to_all(heads_b, "tp", split_axis=0, concat_axis=1, tiled=True),
    )
    joined = jnp.concatenate([back_a.reshape(tok_dev, -1), back_b.reshape(tok_dev, -1)], axis=1)
    project = jnp.dot(joined, out_weight, preferred_element_type=jnp.float32)
    middle = (resid.astype(jnp.float32) + project).astype(jnp.bfloat16)
    middle_f = middle.astype(jnp.float32)
    normed = (
        middle_f
        * lax.rsqrt(jnp.mean(middle_f * middle_f, axis=1, keepdims=True) + EPSILON)
        * norm_gain[None, :]
    ).astype(jnp.bfloat16)
    shared = swiglu_rows(normed, shared_gate, shared_up, shared_down)
    top_count = expert_ids.shape[1]
    model_width = normed.shape[1]
    sp_count = lax.axis_size("sp")
    tp_count = lax.axis_size("tp")
    expert_total = sp_count * tp_count
    pair_count = tok_dev * top_count
    capacity = max(2, 2 * pair_count // expert_total)
    flat_ids = expert_ids.reshape(-1)
    one_hot = (flat_ids[:, None] == jnp.arange(expert_total, dtype=jnp.int32)[None, :]).astype(
        jnp.int32
    )
    pair_rank = jnp.sum((jnp.cumsum(one_hot, axis=0) - one_hot) * one_hot, axis=1)
    pair_token = jnp.arange(pair_count, dtype=jnp.int32) // top_count
    send_rows = (
        jnp.zeros((expert_total, capacity, model_width), jnp.bfloat16)
        .at[flat_ids, pair_rank]
        .set(normed[pair_token])
    )
    arrived = lax.all_to_all(send_rows, ("sp", "tp"), split_axis=0, concat_axis=0, tiled=True)
    arrived_shape = arrived.shape
    flat_rows = arrived.reshape(-1, arrived_shape[-1])
    result = swiglu_rows(flat_rows, gate_experts[0], up_experts[0], down_experts[0]).astype(
        jnp.bfloat16
    )
    finished = result.reshape(arrived_shape)
    returned = lax.all_to_all(finished, ("sp", "tp"), split_axis=0, concat_axis=0, tiled=True)
    chosen = returned[flat_ids, pair_rank].reshape(tok_dev, top_count, model_width)
    routed = jnp.sum(chosen.astype(jnp.float32) * expert_mix[:, :, None], axis=1)
    return (middle_f + shared + routed).astype(jnp.bfloat16)


def solution(mesh):
    in_specs = (
        P(("sp", "tp"), None),
        P("sp", "tp", None),
        P("sp", "tp", None),
        P("sp", "tp", None),
        P("sp", "tp", None),
        P("sp", "tp", None),
        P("sp", "tp", None),
        P("tp"),
        P("tp"),
        P(),
        P(),
        P(),
        P(("sp", "tp"), None),
        P(("sp", "tp"), None),
        P(("sp", "tp"), None, None),
        P(("sp", "tp"), None, None),
        P(("sp", "tp"), None, None),
        P(),
        P(),
        P(),
    )
    out_specs = P(("sp", "tp"), None)
    return jax.shard_map(
        per_device, mesh=mesh, in_specs=in_specs, out_specs=out_specs, check_vma=False
    )
```

profile of v0, /device:TPU:0, one launch (start us, length us, event | category | flops | bytes accessed | tf_op | source)
XLA Modules:
  0.0 333.9 jit_solution(18437636033774966400)
XLA Ops:
  7.3 33.6 %all_gather.12 = bf16[2048,1,128]{2,0,1:T(8,128)(2,1)S(1)} all-gather(bf16[256,1,128]{2,0,1:T(8,128)(2,1)} %param.22), channel_id=1, replica_groups=mesh['sp'=8,'tp'=4] {'sp'}, dimensions={0}, use_global_device_ids=true | all-gather | bytes 589824 | tf_op jit(solution)/shard_map/all_gather | solution.py:107
  44.2 2.8 fusion.88
  47.0 1.8 fusion.89
  48.9 31.4 %all_gather.15 = bf16[2048,1,128]{2,0,1:T(8,128)(2,1)S(1)} all-gather(bf16[256,1,128]{2,0,1:T(8,128)(2,1)S(1)} %copy-done.5), channel_id=1, replica_groups=mesh['sp'=8,'tp'=4] {'sp'}, dimensions={0}, use_global_device_ids=true | all-gather | bytes 589824 | tf_op jit(solution)/shard_map/all_gather | solution.py:110
  80.3 31.5 %all_gather.13 = bf16[2048,1,128]{2,0,1:T(8,128)(2,1)S(1)} all-gather(bf16[256,1,128]{2,0,1:T(8,128)(2,1)S(1)} %copy-done.6), channel_id=1, replica_groups=mesh['sp'=8,'tp'=4] {'sp'}, dimensions={0}, use_global_device_ids=true | all-gather | bytes 589824 | tf_op jit(solution)/shard_map/all_gather | solution.py:108
  111.8 1.8 fusion.91
  115.4 2.1 fusion.19
  122.5 3.3 all-to-all-start.1
  127.3 2.6 all-to-all-done.1
  129.9 3.3 all-to-all-start
  133.3 3.9 %all-to-all-done = bf16[4,2,4096]{2,1,0:T(2,128)(2,1)S(1)} async-done(((bf16[4,2,4096]{2,1,0:T(2,128)(2,1)}), bf16[4,2,4096]{2,1,0:T(2,128)(2,1)S(1)}, u32[]{:S(2)}, u32[]{:S(2)}) %all-to-all-start) | async-done | bytes 65568 | tf_op jit(solution)/shard_map/all_to_all | solution.py:139
  137.4 3.2 multiply_reduce_fusion.1
  140.7 2.3 gather_fusion
  144.7 46.2 %scatter_fusion = bf16[32,16,2048]{2,1,0:T(8,128)(2,1)} fusion(bf16[32,16,2048]{2,1,0:T(8,128)(2,1)} %broadcast_in_dim.49, s32[256]{0:T(256)S(1)} %bitcast.169, bf16[256,2048]{1,0:T(8,128)(2,1)} %gather_fusion), kind=kCustom, calls=%fused_computation.2 | custom fusion | bytes 3147776 | tf_op jit(solution)/shard_map/scatter | solution.py:168
  190.9 53.7 %all_to_all.40 = bf16[32,16,2048]{2,1,0:T(8,128)(2,1)S(1)} all-to-all(bf16[32,16,2048]{2,1,0:T(8,128)(2,1)} %scatter_fusion), channel_id=1, replica_groups=mesh['sp'=8,'tp'=4] {'sp','tp'}, dimensions={0} | all-to-all | bytes 4194304 | tf_op jit(solution)/shard_map/all_to_all | solution.py:170
  246.0 3.6 %fusion.4 = f32[512,1024]{1,0:T(8,128)} fusion(bf16[512,2048]{1,0:T(8,128)(2,1)S(1)} %bitcast.171, bf16[1,2048,1024]{2,1,0:T(8,128)(2,1)S(1)} %copy-done.10), kind=kOutput, calls=%fused_computation.7 | convolution fusion | flops 2147483648 | bytes 8388608 | tf_op jit(solution)/shard_map/dot_general | solution.py:14
  249.6 10.6 %fusion.6 = bf16[512,2048]{1,0:T(8,128)(2,1)} fusion(bf16[1,1024,2048]{2,1,0:T(8,128)(2,1)} %param.36, f32[512,1024]{1,0:T(8,128)} %fusion.4, bf16[512,2048]{1,0:T(8,128)(2,1)} %bitcast.172, bf16[1,2048,1024]{2,1,0:T(8,128)(2,1)} %param.35), kind=kOutput, calls=%fused_computation.9 | convolution fusion | flops 4299161600 | bytes 14680064 | tf_op jit(solution)/shard_map/dot_general | solution.py:17
  260.2 3.8 %all-to-all-start.3 = ((bf16[32,16,2048]{2,1,0:T(8,128)(2,1)}), bf16[32,16,2048]{2,1,0:T(8,128)(2,1)}, u32[]{:S(2)}, u32[]{:S(2)}) async-start(bf16[32,16,2048]{2,1,0:T(8,128)(2,1)} %bitcast.170), calls=%async_computation.3 | async-start | bytes 4194304 | tf_op jit(solution)/shard_map/all_to_all | solution.py:177
  264.7 2.1 fusion.92
  266.8 45.9 %all-to-all-done.3 = bf16[32,16,2048]{2,1,0:T(8,128)(2,1)} async-done(((bf16[32,16,2048]{2,1,0:T(8,128)(2,1)}), bf16[32,16,2048]{2,1,0:T(8,128)(2,1)}, u32[]{:S(2)}, u32[]{:S(2)}) %all-to-all-start.3) | async-done | bytes 2097184 | tf_op jit(solution)/shard_map/all_to_all | solution.py:177
  312.7 5.1 %gather_fusion.1 = bf16[256,2048]{1,0:T(8,128)(2,1)} fusion(bf16[32,16,2048]{2,1,0:T(8,128)(2,1)} %all-to-all-done.3, s32[256]{0:T(256)S(1)} %bitcast.168), kind=kCustom, calls=%fused_computation.1 | custom fusion | bytes 2099200 | tf_op jit(solution)/shard_map/gather | solution.py:178
  317.9 2.7 reshape.410
  320.6 3.2 multiply_reduce_fusion
  323.8 3.2 fusion.14
  (76 shorter events, 15.0 us)
Async XLA Ops:
  6.5 317.3 %copy-start = (bf16[512,2048]{1,0:T(8,128)(2,1)S(1)}, bf16[512,2048]{1,0:T(8,128)(2,1)}, u32[]{:S(2)}) copy-start(bf16[512,2048]{1,0:T(8,128)(2,1)} %param.39) | copy-start | bytes 6291460
  6.5 40.5 %copy-start.12 = (bf16[256,1,128]{2,0,1:T(8,128)(2,1)S(1)}, bf16[256,1,128]{2,0,1:T(8,128)(2,1)}, u32[]{:S(2)}) copy-start(bf16[256,1,128]{2,0,1:T(8,128)(2,1)} %param.21) | copy-start | bytes 196612
  6.5 105.2 %all-gather.2.cloned.1.call-start = ((), (), s32[]{:S(2)}) async-start(), calls=%async_computation.4 | async-start | bytes 1179648 | tf_op jit(solution)/shard_map/all_gather | solution.py:109
  47.0 1.9 copy-start.5
  47.0 33.3 %copy-start.6 = (bf16[256,1,128]{2,0,1:T(8,128)(2,1)S(1)}, bf16[256,1,128]{2,0,1:T(8,128)(2,1)}, u32[]{:S(2)}) copy-start(bf16[256,1,128]{2,0,1:T(8,128)(2,1)} %param.23) | copy-start | bytes 196612
  47.0 64.8 %copy-start.11 = (bf16[256,1,256]{2,0,1:T(8,128)(2,1)S(1)}, bf16[256,1,256]{2,0,1:T(8,128)(2,1)}, u32[]{:S(2)}) copy-start(bf16[256,1,256]{2,0,1:T(8,128)(2,1)} %param.24) | copy-start | bytes 393220
  111.8 3.6 %copy-start.2 = (f32[256,2048]{1,0:T(8,128)S(1)}, f32[256,2048]{1,0:T(8,128)}, u32[]{:S(2)}) copy-start(f32[256,2048]{1,0:T(8,128)} %get-tuple-element.62) | copy-start | bytes 6291460
  113.6 1.8 copy-start.1
  119.6 0.7 copy-start.9
  120.3 17.1 %copy-start.4 = (bf16[64,2048]{1,0:T(8,128)(2,1)S(1)}, bf16[64,2048]{1,0:T(8,128)(2,1)}, u32[]{:S(2)}) copy-start(bf16[64,2048]{1,0:T(8,128)(2,1)} %param.20) | copy-start | bytes 786436
  122.5 7.4 %all-to-all-start.1 = ((bf16[4,2,4096]{2,1,0:T(2,128)(2,1)}), bf16[4,2,4096]{2,1,0:T(2,128)(2,1)S(1)}, u32[]{:S(2)}, u32[]{:S(2)}) async-start(bf16[4,2,4096]{2,1,0:T(2,128)(2,1)} %reshape.432), calls=%async_computation.1 | async-start | bytes 131072 | tf_op jit(solution)/shard_map/all_to_all | solution.py:140
  129.9 7.4 %all-to-all-start = ((bf16[4,2,4096]{2,1,0:T(2,128)(2,1)}), bf16[4,2,4096]{2,1,0:T(2,128)(2,1)S(1)}, u32[]{:S(2)}, u32[]{:S(2)}) async-start(bf16[4,2,4096]{2,1,0:T(2,128)(2,1)} %reshape.434), calls=%async_computation | async-start | bytes 131072 | tf_op jit(solution)/shard_map/all_to_all | solution.py:139
  137.4 3.2 copy-start.7
  190.9 55.0 %copy-start.10 = (bf16[1,2048,1024]{2,1,0:T(8,128)(2,1)S(1)}, bf16[1,2048,1024]{2,1,0:T(8,128)(2,1)}, u32[]{:S(2)}) copy-start(bf16[1,2048,1024]{2,1,0:T(8,128)(2,1)} %param.34) | copy-start | bytes 12582916
  244.6 1.3 copy-start.3
  260.2 3.8 %copy-start.8 = (f32[64,4]{0,1:T(4,128)S(1)}, f32[64,4]{0,1:T(4,128)}, u32[]{:S(2)}) copy-start(f32[64,4]{0,1:T(4,128)} %param.33) | copy-start | bytes 3076
  260.2 52.5 %all-to-all-start.3 = ((bf16[32,16,2048]{2,1,0:T(8,128)(2,1)}), bf16[32,16,2048]{2,1,0:T(8,128)(2,1)}, u32[]{:S(2)}, u32[]{:S(2)}) async-start(bf16[32,16,2048]{2,1,0:T(8,128)(2,1)} %bitcast.170), calls=%async_computation.3 | async-start | bytes 4194304 | tf_op jit(solution)/shard_map/all_to_all | solution.py:177
Sparse Core Ops, SparseCore 0:
  9.5 43.6 all-gather.1
where the time goes:
time: 336 us; the launch traced here: 334 us
  blocking collectives  150 us (45%)
  local copies, waits for them, and re-layouts  63.9 us (19%)
  waiting for transfers between devices  53.1 us (16%)
  matrix products  33.6 us (10%)
  between operations  15.1 us (4%)
  starting transfers between devices  10.4 us (3%)
  other arithmetic  7.7 us (2%)
    all_to_all x1, blocking collectives, per_device(): lax.all_to_all(send_rows, ('sp', 'tp'), split_axis=0, concat_axis=0, tile...  53.7 us
    scatter x1, local copies, waits for them, and re-layouts, per_device(): send_rows = jnp.zeros((expert_total, capacity, model_width), jnp.bfloat16...  46.2 us
    all_to_all x1, waiting for transfers between devices, per_device(): lax.all_to_all(finished, ('sp', 'tp'), split_axis=0, concat_axis=0, tiled...  45.9 us
    all_gather x1, blocking collectives, per_device(): key_piece_a = lax.all_gather(key_a, 'sp', axis=0, tiled=True)  33.6 us
    all_gather x1, blocking collectives, per_device(): value_piece_a = lax.all_gather(value_a, 'sp', axis=0, tiled=True)  31.5 us
    all_gather x1, blocking collectives, per_device(): value_piece_b = lax.all_gather(value_b, 'sp', axis=0, tiled=True)  31.4 us
    dot_general x2, matrix products, swiglu_rows(): return jnp.dot(hidden, w_down, preferred_element_type=jnp.float32)  13.8 us
    dot_general x4, matrix products, online_update(): jnp.einsum('qhd,khd->hqk', query_map, key_map, preferred_element_type=jnp...  8.17 us
  transfers between devices with their start and end apart: 4, of which 3 were waited for; matrix products, arithmetic and copies ran while one was open for 3% of the time, Pallas kernels for 0%

commit v1 on v0

--- a/solution.py
+++ b/solution.py
@@ -104,8 +104,11 @@
         empty_state(query_rows, query_a.shape[1], value_width),
         empty_state(query_rows, query_b.shape[1], value_width),
     )
-    key_piece_a = lax.all_gather(key_a, "sp", axis=0, tiled=True)
-    value_piece_a = lax.all_gather(value_a, "sp", axis=0, tiled=True)
+    key_piece_a, value_piece_a = jnp.split(
+        lax.all_gather(jnp.concatenate([key_a, value_a], axis=1), "sp", axis=0, tiled=True),
+        [key_a.shape[1]],
+        axis=1,
+    )
     key_piece_b = lax.all_gather(key_b, "sp", axis=0, tiled=True)
     value_piece_b = lax.all_gather(value_b, "sp", axis=0, tiled=True)
     piece_rows = key_piece_a.shape[0]

time: 336 us -> 317 us (0.943)
  blocking collectives: 150 us -> 86.2 us
  waiting for transfers between devices: 53.1 us -> 97.3 us
    all_gather x2 -> x0, blocking collectives: 65.1 us -> none  [the longest x1 33.6 us: per_device(): key_piece_a = lax.all_gather(key_a, 'sp', axis=0, tiled=True)]
    all_gather x1, waiting for transfers between devices: 0.01 us -> 36.3 us  [per_device(): key_piece_b = lax.all_gather(key_b, 'sp', axis=0, tiled=True)]
    all_gather x0 -> x1, waiting for transfers between devices: none -> 7.84 us  [per_device(): lax.all_gather(jnp.concatenate([key_a, value_a], axis=1), 'sp', axis=0, t...]
  transfers between devices with their start and end apart: 4 -> 5, of which waited for: 3 -> 5; matrix products, arithmetic and copies ran while one was open for 3% -> 4% of each run, Pallas kernels for 0% -> 0%
where the time goes in v1:
time: 317 us; the launch traced here: 316 us
  waiting for transfers between devices  97.3 us (31%)
  blocking collectives  86.2 us (27%)
  local copies, waits for them, and re-layouts  64.5 us (20%)
  matrix products  33.2 us (10%)
  between operations  15.1 us (5%)
  starting transfers between devices  10.3 us (3%)
  other arithmetic  8.82 us (3%)
    all_to_all x1, blocking collectives, per_device(): lax.all_to_all(send_rows, ('sp', 'tp'), split_axis=0, concat_axis=0, tile...  51.9 us
    scatter x1, local copies, waits for them, and re-layouts, per_device(): send_rows = jnp.zeros((expert_total, capacity, model_width), jnp.bfloat16...  46.2 us
    all_to_all x1, waiting for transfers between devices, per_device(): lax.all_to_all(finished, ('sp', 'tp'), split_axis=0, concat_axis=0, tiled...  45.9 us
    all_gather x1, waiting for transfers between devices, per_device(): key_piece_b = lax.all_gather(key_b, 'sp', axis=0, tiled=True)  36.3 us
    all_gather x1, blocking collectives, per_device(): value_piece_b = lax.all_gather(value_b, 'sp', axis=0, tiled=True)  34.4 us
    dot_general x2, matrix products, swiglu_rows(): return jnp.dot(hidden, w_down, preferred_element_type=jnp.float32)  13.8 us
    dot_general x4, matrix products, online_update(): jnp.einsum('qhd,khd->hqk', query_map, key_map, preferred_element_type=jnp...  8.31 us
    all_gather x1, waiting for transfers between devices, per_device(): lax.all_gather(jnp.concatenate([key_a, value_a], axis=1), 'sp', axis=0, t...  7.84 us
  transfers between devices with their start and end apart: 5, of which 5 were waited for; matrix products, arithmetic and copies ran while one was open for 4% of the time, Pallas kernels for 0%

profile of v1, /device:TPU:0, one launch (start us, length us, event | category | flops | bytes accessed | tf_op | source)
XLA Modules:
  0.0 315.5 jit_solution(1134472638227759348)
XLA Ops:
  12.4 34.4 %all_gather.11 = bf16[2048,1,128]{2,0,1:T(8,128)(2,1)S(1)} all-gather(bf16[256,1,128]{2,0,1:T(8,128)(2,1)} %param.26), channel_id=1, replica_groups=mesh['sp'=8,'tp'=4] {'sp'}, dimensions={0}, use_global_device_ids=true | all-gather | bytes 589824 | tf_op jit(solution)/shard_map/all_gather | solution.py:113
  46.7 7.8 %all-gather.3.cloned.1.call-done = bf16[2048,2,128]{2,0,1:T(8,128)(2,1)} async-done(((bf16[256,2,128]{2,0,1:T(8,128)(2,1)}), bf16[2048,2,128]{2,0,1:T(8,128)(2,1)}) %all-gather.3.cloned.1.call-update) | async-done | bytes 1048592 | tf_op jit(solution)/shard_map/all_gather | solution.py:108
  54.6 3.1 fusion.94
  57.7 1.8 fusion.95
  59.5 36.3 %all-gather.5.cloned.1.call-done = bf16[2048,1,256]{2,0,1:T(8,128)(2,1)} async-done(((bf16[256,1,256]{2,0,1:T(8,128)(2,1)}), bf16[2048,1,256]{2,0,1:T(8,128)(2,1)}) %all-gather.5.cloned.1.call-update) | async-done | bytes 1048592 | tf_op jit(solution)/shard_map/all_gather | solution.py:112
  95.8 1.7 fusion.97
  97.5 1.7 fusion.96
  106.0 3.3 %all-to-all-start.1 = ((bf16[4,2,4096]{2,1,0:T(2,128)(2,1)}), bf16[4,2,4096]{2,1,0:T(2,128)(2,1)S(1)}, u32[]{:S(2)}, u32[]{:S(2)}) async-start(bf16[4,2,4096]{2,1,0:T(2,128)(2,1)} %reshape.432), calls=%async_computation.1 | async-start | bytes 131072 | tf_op jit(solution)/shard_map/all_to_all | solution.py:143
  110.8 2.6 all-to-all-done.1
  113.4 3.3 %all-to-all-start = ((bf16[4,2,4096]{2,1,0:T(2,128)(2,1)}), bf16[4,2,4096]{2,1,0:T(2,128)(2,1)S(1)}, u32[]{:S(2)}, u32[]{:S(2)}) async-start(bf16[4,2,4096]{2,1,0:T(2,128)(2,1)} %reshape.434), calls=%async_computation | async-start | bytes 131072 | tf_op jit(solution)/shard_map/all_to_all | solution.py:142
  116.8 3.9 %all-to-all-done = bf16[4,2,4096]{2,1,0:T(2,128)(2,1)S(1)} async-done(((bf16[4,2,4096]{2,1,0:T(2,128)(2,1)}), bf16[4,2,4096]{2,1,0:T(2,128)(2,1)S(1)}, u32[]{:S(2)}, u32[]{:S(2)}) %all-to-all-start) | async-done | bytes 65568 | tf_op jit(solution)/shard_map/all_to_all | solution.py:142
  120.9 3.2 %multiply_reduce_fusion.1 = (f32[64]{0:T(128)S(1)}, f32[64,2048]{1,0:T(8,128)S(1)}) fusion(bf16[1024,2048]{1,0:T(8,128)(2,1)} %param.30, bf16[64,512]{1,0:T(8,128)(2,1)S(1)} %bitcast.176, bf16[64,512]{1,0:T(8,128)(2,1)S(1)} %bitcast.177, bf16[64,2048]{1,0:T(8,128)(2,1)S(1)} %copy-done.4), kind=kOutput, calls=%fused_computation.75 | convolution fusion | flops 269483968 | bytes 5112064 | tf_op jit(solution)/shard_map/dot_general | solution.py:146
  124.2 2.3 gather_fusion
  128.2 46.2 %scatter_fusion = bf16[32,16,2048]{2,1,0:T(8,128)(2,1)} fusion(bf16[32,16,2048]{2,1,0:T(8,128)(2,1)} %broadcast_in_dim.49, s32[256]{0:T(256)S(1)} %bitcast.172, bf16[256,2048]{1,0:T(8,128)(2,1)} %gather_fusion), kind=kCustom, calls=%fused_computation.2 | custom fusion | bytes 3147776 | tf_op jit(solution)/shard_map/scatter | solution.py:171
  174.4 51.9 %all_to_all.40 = bf16[32,16,2048]{2,1,0:T(8,128)(2,1)S(1)} all-to-all(bf16[32,16,2048]{2,1,0:T(8,128)(2,1)} %scatter_fusion), channel_id=1, replica_groups=mesh['sp'=8,'tp'=4] {'sp','tp'}, dimensions={0} | all-to-all | bytes 4194304 | tf_op jit(solution)/shard_map/all_to_all | solution.py:173
  227.7 3.6 %fusion.4 = f32[512,1024]{1,0:T(8,128)} fusion(bf16[512,2048]{1,0:T(8,128)(2,1)S(1)} %bitcast.174, bf16[1,2048,1024]{2,1,0:T(8,128)(2,1)S(1)} %copy-done.8), kind=kOutput, calls=%fused_computation.7 | convolution fusion | flops 2147483648 | bytes 8388608 | tf_op jit(solution)/shard_map/dot_general | solution.py:14
  231.3 10.6 %fusion.6 = bf16[512,2048]{1,0:T(8,128)(2,1)} fusion(bf16[1,1024,2048]{2,1,0:T(8,128)(2,1)} %param.36, f32[512,1024]{1,0:T(8,128)} %fusion.4, bf16[512,2048]{1,0:T(8,128)(2,1)} %bitcast.175, bf16[1,2048,1024]{2,1,0:T(8,128)(2,1)} %param.35), kind=kOutput, calls=%fused_computation.9 | convolution fusion | flops 4299161600 | bytes 14680064 | tf_op jit(solution)/shard_map/dot_general | solution.py:17
  241.9 3.7 %all-to-all-start.3 = ((bf16[32,16,2048]{2,1,0:T(8,128)(2,1)}), bf16[32,16,2048]{2,1,0:T(8,128)(2,1)}, u32[]{:S(2)}, u32[]{:S(2)}) async-start(bf16[32,16,2048]{2,1,0:T(8,128)(2,1)} %bitcast.173), calls=%async_computation.3 | async-start | bytes 4194304 | tf_op jit(solution)/shard_map/all_to_all | solution.py:180
  246.3 2.1 fusion.98
  248.4 45.9 %all-to-all-done.3 = bf16[32,16,2048]{2,1,0:T(8,128)(2,1)} async-done(((bf16[32,16,2048]{2,1,0:T(8,128)(2,1)}), bf16[32,16,2048]{2,1,0:T(8,128)(2,1)}, u32[]{:S(2)}, u32[]{:S(2)}) %all-to-all-start.3) | async-done | bytes 2097184 | tf_op jit(solution)/shard_map/all_to_all | solution.py:180
  294.3 5.1 %gather_fusion.1 = bf16[256,2048]{1,0:T(8,128)(2,1)} fusion(bf16[32,16,2048]{2,1,0:T(8,128)(2,1)} %all-to-all-done.3, s32[256]{0:T(256)S(1)} %bitcast.171), kind=kCustom, calls=%fused_computation.1 | custom fusion | bytes 2099200 | tf_op jit(solution)/shard_map/gather | solution.py:181
  299.5 2.7 reshape.410
  302.2 3.2 %multiply_reduce_fusion = f32[64,2048]{1,0:T(8,128)S(1)} fusion(f32[64,4,2048]{2,1,0:T(4,128)} %reshape.410, f32[64,4]{1,0:T(8,128)} %copy.45), kind=kLoop, calls=%fused_computation.26 | loop fusion | flops 917504 | bytes 2622464 | tf_op jit(solution)/shard_map/reduce_sum | solution.py:182
  305.4 3.2 %fusion.16 = bf16[64,2048]{1,0:T(8,128)(2,1)} fusion(f32[64,2048]{1,0:T(8,128)S(1)} %multiply_reduce_fusion, f32[64,2048]{1,0:T(8,128)S(1)} %get-tuple-element.97, bf16[512,2048]{1,0:T(8,128)(2,1)S(1)} %copy-done, bf16[64,2048]{1,0:T(8,128)(2,1)S(1)} %multiply_convert_fusion.1, bf16[2048,512]{1,0:T(8,128)(2,1)} %param.38, f32[64,512]{1,0:T(8,128)S(1)} %fusion.98), kind=kOutput, calls=%fused_computation.23 | convolution fusion | flops 269025280 | bytes 5898240 | tf_op jit(solution)/shard_map/dot_general | solution.py:17
  (78 shorter events, 16.6 us)
Async XLA Ops:
  6.5 298.9 %copy-start = (bf16[512,2048]{1,0:T(8,128)(2,1)S(1)}, bf16[512,2048]{1,0:T(8,128)(2,1)}, u32[]{:S(2)}) copy-start(bf16[512,2048]{1,0:T(8,128)(2,1)} %param.39) | copy-start | bytes 6291460
  6.5 48.0 %all-gather.3.cloned.1.call-start = ((), (), s32[]{:S(2)}) async-start(), calls=%async_computation.4 | async-start | bytes 1179648 | tf_op jit(solution)/shard_map/all_gather | solution.py:108
  8.2 49.4 %copy-start.12 = (bf16[256,1,128]{2,0,1:T(8,128)(2,1)S(1)}, bf16[256,1,128]{2,0,1:T(8,128)(2,1)}, u32[]{:S(2)}) copy-start(bf16[256,1,128]{2,0,1:T(8,128)(2,1)} %param.21) | copy-start | bytes 196612
  8.3 87.5 %all-gather.5.cloned.1.call-start = ((), (), s32[]{:S(2)}) async-start(), calls=%async_computation.5 | async-start | bytes 1179648 | tf_op jit(solution)/shard_map/all_gather | solution.py:112
  54.6 3.1 copy-start.9
  57.6 38.2 %copy-start.11 = (bf16[256,1,256]{2,0,1:T(8,128)(2,1)S(1)}, bf16[256,1,256]{2,0,1:T(8,128)(2,1)}, u32[]{:S(2)}) copy-start(bf16[256,1,256]{2,0,1:T(8,128)(2,1)} %param.24) | copy-start | bytes 393220
  95.8 3.5 %copy-start.2 = (f32[256,2048]{0,1:T(8,128)S(1)}, f32[256,2048]{0,1:T(8,128)}, u32[]{:S(2)}) copy-start(f32[256,2048]{0,1:T(8,128)} %get-tuple-element.62) | copy-start | bytes 6291460
  97.5 1.8 copy-start.1
  101.4 1.2 copy-start.10
  103.1 0.7 copy-start.7
  103.7 17.2 %copy-start.4 = (bf16[64,2048]{1,0:T(8,128)(2,1)S(1)}, bf16[64,2048]{1,0:T(8,128)(2,1)}, u32[]{:S(2)}) copy-start(bf16[64,2048]{1,0:T(8,128)(2,1)} %param.20) | copy-start | bytes 786436
  106.0 7.4 %all-to-all-start.1 = ((bf16[4,2,4096]{2,1,0:T(2,128)(2,1)}), bf16[4,2,4096]{2,1,0:T(2,128)(2,1)S(1)}, u32[]{:S(2)}, u32[]{:S(2)}) async-start(bf16[4,2,4096]{2,1,0:T(2,128)(2,1)} %reshape.432), calls=%async_computation.1 | async-start | bytes 131072 | tf_op jit(solution)/shard_map/all_to_all | solution.py:143
  113.4 7.4 %all-to-all-start = ((bf16[4,2,4096]{2,1,0:T(2,128)(2,1)}), bf16[4,2,4096]{2,1,0:T(2,128)(2,1)S(1)}, u32[]{:S(2)}, u32[]{:S(2)}) async-start(bf16[4,2,4096]{2,1,0:T(2,128)(2,1)} %reshape.434), calls=%async_computation | async-start | bytes 131072 | tf_op jit(solution)/shard_map/all_to_all | solution.py:142
  120.9 3.2 %copy-start.5 = (f32[2048]{0:T(1024)S(1)}, f32[2048]{0:T(1024)}, u32[]{:S(2)}) copy-start(f32[2048]{0:T(1024)} %param.31) | copy-start | bytes 24580
  174.4 53.2 %copy-start.8 = (bf16[1,2048,1024]{2,1,0:T(8,128)(2,1)S(1)}, bf16[1,2048,1024]{2,1,0:T(8,128)(2,1)}, u32[]{:S(2)}) copy-start(bf16[1,2048,1024]{2,1,0:T(8,128)(2,1)} %param.34) | copy-start | bytes 12582916
  226.3 1.3 copy-start.3
  241.9 3.7 %copy-start.6 = (f32[64,4]{0,1:T(4,128)S(1)}, f32[64,4]{0,1:T(4,128)}, u32[]{:S(2)}) copy-start(f32[64,4]{0,1:T(4,128)} %param.33) | copy-start | bytes 3076
  241.9 52.4 %all-to-all-start.3 = ((bf16[32,16,2048]{2,1,0:T(8,128)(2,1)}), bf16[32,16,2048]{2,1,0:T(8,128)(2,1)}, u32[]{:S(2)}, u32[]{:S(2)}) async-start(bf16[32,16,2048]{2,1,0:T(8,128)(2,1)} %bitcast.173), calls=%async_computation.3 | async-start | bytes 4194304 | tf_op jit(solution)/shard_map/all_to_all | solution.py:180
Sparse Core Ops, SparseCore 0:
  9.5 44.9 all-gather.2
  56.7 39.0 all-gather.4
